TPU v7x, 32 devices: a whole 2x2x4 slice. The times are simulated.
32 devices in a mesh: sp: 8 (over z, x), dp: 4 (over y, core).
Axes of the slice: x: 2, y: 2, z: 4, core: 2. Of those that a mesh axis runs over, the one named last changes fastest.
Arguments:
- queries: bfloat16 [4, 1024, 16, 128], P('dp', 'sp'), may hold values from -6 to 6
- key_rows: bfloat16 [4, 1024, 4, 128], P('dp', 'sp'), may hold values from -6 to 6
- values: bfloat16 [4, 1024, 4, 128], P('dp', 'sp'), may hold values from -6 to 6
- query_gain: float32 [128], replicated, may hold values from 0.4 to 5
- key_gain: float32 [128], replicated, may hold values from 0.4 to 5
- out_weight: bfloat16 [2048, 2048], P('sp', 'dp'), may hold values from -0.125 to 0.125
- residual: bfloat16 [4, 1024, 2048], P('dp', 'sp'), may hold values from -6 to 6
- norm_gain: float32 [2048], replicated, may hold values from 0.1 to 1.9
- expert_gate: bfloat16 [8, 2048, 1792], P('sp'), may hold values from -0.125 to 0.125
- expert_up: bfloat16 [8, 2048, 1792], P('sp'), may hold values from -0.125 to 0.125
- expert_down: bfloat16 [8, 1792, 2048], P('sp'), may hold values from -0.125 to 0.125
- routes: int32 [4, 1024, 2], P('dp', 'sp'), may hold values from 0 to 7, all different within a row; in each aligned block of 64 rows (0 to 63, 64 to 127, ..., all dimensions but the last counted through in order) at most 32 rows name the same one
- route_weight: float32 [4, 1024, 2], P('dp', 'sp'), may hold values from 0.25 to 1
Outputs:
- layer_out: bfloat16 [4, 1024, 2048], P('dp', 'sp')
Inputs may be any that keep to these rules, and one draw needn't show every extreme that they name: `routes`: in each aligned block of 64 rows of one device, no expert is named by more than 32 entries, a bound that some block reaches; the two experts of a row differ.
All inputs are finite; a program needn't handle non-finite values.
Results may differ from a plain program's by a relative error of at most 0.0095.
The roundings to bfloat16 on the way count: a program that leaves them out, or rounds other values in their place, can miss the bound.
Values may be sent and summed in bfloat16 or wider, within the bound.
No kernel may reach another device: no remote copies, remote signals or barrier semaphores. Data moves between devices by JAX's collectives and lax.ppermute only.
A program may use at most 128 MiB of HBM per device.

v0:
```python
import jax
import jax.numpy as jnp
from jax import lax
from jax.sharding import PartitionSpec as P

GRID_W = 64
EPS = 1e-06
THETA = 10000.0


def rotate_half(vector, position):
    half_size = vector.shape[-1] // 2
    inverse = THETA ** (-jnp.arange(half_size, dtype=jnp.float32) / half_size)
    angles = position[:, None] * inverse[None, :]
    cosine = jnp.cos(angles)[:, None, :]
    sine_part = jnp.sin(angles)[:, None, :]
    first_part = vector[..., :half_size]
    second_part = vector[..., half_size:]
    return jnp.concatenate(
        [
            first_part * cosine - second_part * sine_part,
            first_part * sine_part + second_part * cosine,
        ],
        axis=-1,
    )


def normalize_rotate(vector, gain, positions):
    as_float = vector.astype(jnp.float32)
    scaled = (
        as_float * lax.rsqrt(jnp.mean(as_float * as_float, axis=-1, keepdims=True) + EPS) * gain
    )
    grid_row = (positions // GRID_W).astype(jnp.float32)
    column = (positions % GRID_W).astype(jnp.float32)
    quarter = scaled.shape[-1] // 2
    turned = jnp.concatenate(
        [rotate_half(scaled[..., :quarter], grid_row), rotate_half(scaled[..., quarter:], column)],
        axis=-1,
    )
    return turned.astype(jnp.bfloat16)


def softmax_rows(scores):
    row_max = jnp.max(scores, axis=-1, keepdims=True)
    exponent = jnp.exp(scores - row_max)
    return (exponent / jnp.sum(exponent, axis=-1, keepdims=True)).astype(jnp.bfloat16)


def attend_block(query_rows, key_rows, value_rows):
    scores = jnp.einsum(
        "qd,kd->qk", query_rows, key_rows, preferred_element_type=jnp.float32
    ) * query_rows.shape[-1] ** (-0.5)
    weights = softmax_rows(scores)
    return jnp.dot(weights, value_rows, preferred_element_type=jnp.float32).astype(jnp.bfloat16)


def attend_heads(head_query, head_key, head_value):
    length, head_count, head_width = head_query.shape
    block_size = min(512, length)
    outputs = []
    for head_index in range(head_count):
        key_slice = head_key[:, head_index]
        value_slice = head_value[:, head_index]
        query_blocks = head_query[:, head_index].reshape(
            length // block_size, block_size, head_width
        )

        def one_block(query_block):
            return attend_block(query_block, key_slice, value_slice)

        outputs.append(lax.map(one_block, query_blocks).reshape(length, head_width))
    return jnp.stack(outputs, axis=1)


def project_tokens(attended, out_weight):
    all_rows = lax.all_gather(attended[None], "dp", axis=0, tiled=True)
    local_cols = lax.all_gather(out_weight, "sp", axis=0, tiled=True)
    partial_cols = jnp.einsum(
        "std,dc->stc", all_rows, local_cols, preferred_element_type=jnp.float32
    )
    back_cols = lax.all_to_all(
        partial_cols.astype(jnp.bfloat16), "dp", split_axis=0, concat_axis=2, tiled=True
    ).astype(partial_cols.dtype)
    return back_cols[0]


def on_device(
    queries,
    key_rows,
    values,
    query_gain,
    key_gain,
    out_weight,
    residual,
    norm_gain,
    expert_gate,
    expert_up,
    expert_down,
    routes,
    route_weight,
):
    tok_count = queries.shape[1]
    head_count = queries.shape[2]
    head_width = queries.shape[3]
    group_size = head_count // key_rows.shape[2]
    positions = lax.axis_index("sp") * tok_count + jnp.arange(tok_count, dtype=jnp.int32)
    rot_query = normalize_rotate(queries[0], query_gain, positions)
    rot_key = normalize_rotate(key_rows[0], key_gain, positions)
    value_rows = values[0]
    head_query, head_key, head_value = (
        lax.all_to_all(rot_query, "sp", split_axis=1, concat_axis=0, tiled=True),
        lax.all_to_all(
            jnp.repeat(rot_key, group_size, axis=1), "sp", split_axis=1, concat_axis=0, tiled=True
        ),
        lax.all_to_all(
            jnp.repeat(value_rows, group_size, axis=1),
            "sp",
            split_axis=1,
            concat_axis=0,
            tiled=True,
        ),
    )
    by_heads = attend_heads(head_query, head_key, head_value)
    returned_heads = lax.all_to_all(by_heads, "sp", split_axis=0, concat_axis=1, tiled=True)
    projected = project_tokens(
        returned_heads.reshape(tok_count, head_count * head_width), out_weight
    )
    mixed_sum = residual[0].astype(jnp.float32) + projected
    normed = (
        mixed_sum
        * lax.rsqrt(jnp.mean(mixed_sum * mixed_sum, axis=-1, keepdims=True) + EPS)
        * norm_gain
    ).astype(jnp.bfloat16)
    experts = expert_gate.shape[0] * lax.axis_size("sp")
    half_rows = tok_count // 2
    capacity = max(2, 4 * half_rows // experts)
    chosen = routes[0].reshape(2, half_rows * 2)
    onehot = (chosen[..., None] == jnp.arange(experts, dtype=jnp.int32)).astype(jnp.int32)
    slot_rank = jnp.sum(jnp.cumsum(onehot, axis=1) * onehot, axis=-1) - 1
    slot_index = jnp.arange(2, dtype=jnp.int32)[:, None] * capacity + slot_rank
    target = (chosen * (2 * capacity) + slot_index).reshape(-1)
    model_width = normed.shape[1]
    filled = (
        jnp.zeros((experts * 2 * capacity, model_width), jnp.bfloat16)
        .at[target]
        .set(jnp.repeat(normed, 2, axis=0))
    )
    buffer = filled.reshape(experts, 2 * capacity, model_width)
    slot_batch = lax.all_to_all(buffer, "sp", split_axis=0, concat_axis=0, tiled=True)
    sources, slot_count, feature_count = slot_batch.shape
    flat_rows = slot_batch.reshape(sources * slot_count, feature_count)
    gate_part = jnp.dot(flat_rows, expert_gate[0], preferred_element_type=jnp.float32)
    up_part = jnp.dot(flat_rows, expert_up[0], preferred_element_type=jnp.float32)
    hidden = (jax.nn.silu(gate_part) * up_part).astype(jnp.bfloat16)
    expert_result = jnp.dot(hidden, expert_down[0], preferred_element_type=jnp.float32).astype(
        jnp.bfloat16
    )
    served = expert_result.reshape(sources, slot_count, feature_count)
    returned = lax.all_to_all(served, "sp", split_axis=0, concat_axis=0, tiled=True)
    picked = (
        returned.reshape(-1, model_width)[target]
        .astype(jnp.float32)
        .reshape(tok_count, 2, model_width)
    )
    result = mixed_sum + jnp.sum(picked * route_weight[0][..., None], axis=1)
    return result.astype(jnp.bfloat16)[None]


def solution(mesh):
    in_specs = (
        P("dp", "sp", None, None),
        P("dp", "sp", None, None),
        P("dp", "sp", None, None),
        P(),
        P(),
        P("sp", "dp"),
        P("dp", "sp", None),
        P(),
        P("sp", None, None),
        P("sp", None, None),
        P("sp", None, None),
        P("dp", "sp", None),
        P("dp", "sp", None),
    )
    out_specs = P("dp", "sp", None)
    return jax.shard_map(
        on_device, mesh=mesh, in_specs=in_specs, out_specs=out_specs, check_vma=False
    )
```

profile of v0, /device:TPU:0, one launch (start us, length us, event | category | flops | bytes accessed | tf_op | source)
XLA Modules:
  0.0 305.6 jit_solution(6616813318897419317)
XLA Ops:
  11.2 7.3 %all-to-all-start.1 = ((bf16[128,16,128]{2,0,1:T(8,128)(2,1)}), bf16[128,16,128]{2,0,1:T(8,128)(2,1)S(1)}, u32[]{:S(2)}, u32[]{:S(2)}) async-start(bf16[128,16,128]{2,0,1:T(8,128)(2,1)} %bitcast.12), calls=%async_computation.1 | async-start | bytes 1048576 | tf_op jit(solution)/shard_map/all_to_all | solution.py:112
  20.1 1.5 pad_maximum_fusion
  21.6 11.4 %all-to-all-done.1 = bf16[128,16,128]{2,0,1:T(8,128)(2,1)S(1)} async-done(((bf16[128,16,128]{2,0,1:T(8,128)(2,1)}), bf16[128,16,128]{2,0,1:T(8,128)(2,1)S(1)}, u32[]{:S(2)}, u32[]{:S(2)}) %all-to-all-start.1) | async-done | bytes 524320 | tf_op jit(solution)/shard_map/all_to_all | solution.py:112
  33.0 3.6 %all-to-all-start = ((bf16[128,16,128]{2,0,1:T(8,128)(2,1)}), bf16[128,16,128]{2,0,1:T(8,128)(2,1)S(1)}, u32[]{:S(2)}, u32[]{:S(2)}) async-start(bf16[128,16,128]{2,0,1:T(8,128)(2,1)} %pad_maximum_fusion), calls=%async_computation | async-start | bytes 1048576 | tf_op jit(solution)/shard_map/all_to_all | solution.py:111
  36.7 14.6 %all-to-all-done = bf16[128,16,128]{2,0,1:T(8,128)(2,1)S(1)} async-done(((bf16[128,16,128]{2,0,1:T(8,128)(2,1)}), bf16[128,16,128]{2,0,1:T(8,128)(2,1)S(1)}, u32[]{:S(2)}, u32[]{:S(2)}) %all-to-all-start) | async-done | bytes 524320 | tf_op jit(solution)/shard_map/all_to_all | solution.py:111
  52.2 3.6 %all-to-all-start.2 = ((bf16[128,16,128]{2,0,1:T(8,128)(2,1)}), bf16[128,16,128]{2,0,1:T(8,128)(2,1)S(1)}, u32[]{:S(2)}, u32[]{:S(2)}) async-start(bf16[128,16,128]{2,0,1:T(8,128)(2,1)} %bitcast.18), calls=%async_computation.2 | async-start | bytes 1048576 | tf_op jit(solution)/shard_map/all_to_all | solution.py:115
  56.8 13.7 %all-to-all-done.2 = bf16[128,16,128]{2,0,1:T(8,128)(2,1)S(1)} async-done(((bf16[128,16,128]{2,0,1:T(8,128)(2,1)}), bf16[128,16,128]{2,0,1:T(8,128)(2,1)S(1)}, u32[]{:S(2)}, u32[]{:S(2)}) %all-to-all-start.2) | async-done | bytes 524320 | tf_op jit(solution)/shard_map/all_to_all | solution.py:115
  70.6 3.4 %while.20 = (s32[]{:T(128)}, bf16[2,512,128]{2,1,0:T(8,128)(2,1)S(1)}, bf16[2,512,128]{2,1,0:T(8,128)(2,1)S(1)}, bf16[1024,128]{1,0:T(8,128)(2,1)S(1)}, bf16[1024,128]{1,0:T(8,128)(2,1)S(1)}, /*index=5*/s32[]{:T(128)}) while((s32[]{:T(128)}, bf16[2,512,128]{2,1,0:T(8,128)(2,1)S(1)}, bf16[2,512,128]{2,1,0:T(8,128)(2,1)S(1)}, ...), condition=%wide.region_5.6_spmd, body=%wide.region_2.5_spmd.sunk | while | flops 273218560 | bytes 7088205 | solution.py:71
  74.1 3.5 %while.21 = (s32[]{:T(128)}, bf16[2,512,128]{2,1,0:T(8,128)(2,1)S(1)}, bf16[2,512,128]{2,1,0:T(8,128)(2,1)S(1)}, bf16[1024,128]{1,0:T(8,128)(2,1)S(1)}, bf16[1024,128]{1,0:T(8,128)(2,1)S(1)}, /*index=5*/s32[]{:T(128)}) while((s32[]{:T(128)}, bf16[2,512,128]{2,1,0:T(8,128)(2,1)S(1)}, bf16[2,512,128]{2,1,0:T(8,128)(2,1)S(1)}, ...), condition=%wide.region_9.10_spmd, body=%wide.region_6.9_spmd.sunk | while | flops 273218560 | bytes 7088205 | solution.py:71
  78.2 28.0 %all_to_all.88 = bf16[1024,2,128]{2,1,0:T(2,128)(2,1)S(1)} all-to-all(bf16[1024,2,128]{2,1,0:T(2,128)(2,1)S(1)} %copy.114), channel_id=1, replica_groups=mesh['sp'=8,'dp'=4] {'sp'}, dimensions={0} | all-to-all | bytes 1048576 | tf_op jit(solution)/shard_map/all_to_all | solution.py:124
  108.6 5.1 %all-gather.5.cloned.1.call-done = bf16[2048,512]{1,0:T(8,128)(2,1)} async-done(((bf16[256,512]{1,0:T(8,128)(2,1)}), bf16[2048,512]{1,0:T(8,128)(2,1)}) %all-gather.5.cloned.1.call-update) | async-done | bytes 2097168 | tf_op jit(solution)/shard_map/all_gather | solution.py:77
  113.7 23.2 %all-gather.3.cloned.1.call-done = bf16[4,128,2048]{2,1,0:T(8,128)(2,1)} async-done(((bf16[1,128,2048]{2,1,0:T(8,128)(2,1)}), bf16[4,128,2048]{2,1,0:T(8,128)(2,1)}) %all-gather.3.cloned.1.call-update) | async-done | bytes 2097168 | tf_op jit(solution)/shard_map/all_gather | solution.py:76
  136.9 4.3 %fusion.29 = bf16[4,128,512]{2,1,0:T(8,128)(2,1)} fusion(bf16[4,128,2048]{2,1,0:T(8,128)(2,1)} %all-gather.3.cloned.1.call-done, bf16[2048,512]{1,0:T(8,128)(2,1)} %all-gather.5.cloned.1.call-done), kind=kOutput, calls=%fused_computation.41 | convolution fusion | flops 1074003968 | bytes 4718592 | tf_op jit(solution)/shard_map/std,dc->stc/dot_general | solution.py:78
  141.1 3.7 %all-to-all-start.4 = ((bf16[4,128,512]{2,1,0:T(8,128)(2,1)}), bf16[4,128,512]{2,1,0:T(8,128)(2,1)S(1)}, u32[]{:S(2)}, u32[]{:S(2)}) async-start(bf16[4,128,512]{2,1,0:T(8,128)(2,1)} %fusion.29), calls=%async_computation.4 | async-start | bytes 1048576 | tf_op jit(solution)/shard_map/all_to_all | solution.py:81
  144.9 8.5 %all-to-all-done.4 = bf16[4,128,512]{2,1,0:T(8,128)(2,1)S(1)} async-done(((bf16[4,128,512]{2,1,0:T(8,128)(2,1)}), bf16[4,128,512]{2,1,0:T(8,128)(2,1)S(1)}, u32[]{:S(2)}, u32[]{:S(2)}) %all-to-all-start.4) | async-done | bytes 524320 | tf_op jit(solution)/shard_map/all_to_all | solution.py:81
  156.9 3.5 %scatter_custom_fusion = bf16[512,2048]{1,0:T(8,128)(2,1)S(1)} fusion(s32[256]{0:T(256)S(1)} %bitcast.142, bf16[256,2048]{1,0:T(8,128)(2,1)} %reshape.305, bf16[]{:T(256)} %constant.89.clone.1), kind=kCustom, calls=%fused_computation.50 | custom fusion | bytes 2097664 | tf_op jit(solution)/shard_map/scatter | solution.py:146
  160.4 53.4 %all_to_all.89 = bf16[8,64,2048]{2,1,0:T(8,128)(2,1)} all-to-all(bf16[8,64,2048]{2,1,0:T(8,128)(2,1)S(1)} %bitcast.127), channel_id=1, replica_groups=mesh['sp'=8,'dp'=4] {'sp'}, dimensions={0} | all-to-all | bytes 4194304 | tf_op jit(solution)/shard_map/all_to_all | solution.py:149
  213.8 9.5 %fusion.20 = f32[512,1792]{1,0:T(8,128)} fusion(bf16[512,2048]{1,0:T(8,128)(2,1)} %bitcast.41, bf16[1,2048,1792]{2,1,0:T(8,128)(2,1)} %param.25), kind=kOutput, calls=%fused_computation.30 | convolution fusion | flops 3758096384 | bytes 13107200 | tf_op jit(solution)/shard_map/dot_general | solution.py:152
  223.3 17.0 %fusion.24 = bf16[512,2048]{1,0:T(8,128)(2,1)} fusion(bf16[1,1792,2048]{2,1,0:T(8,128)(2,1)} %param.27, f32[512,1792]{1,0:T(8,128)} %fusion.20, bf16[512,2048]{1,0:T(8,128)(2,1)} %bitcast.41, bf16[1,2048,1792]{2,1,0:T(8,128)(2,1)} %param.26), kind=kOutput, calls=%fused_computation.33 | convolution fusion | flops 7522746368 | bytes 22544384 | tf_op jit(solution)/shard_map/dot_general | solution.py:155
  240.3 4.0 %all-to-all-start.6 = ((bf16[8,64,2048]{2,1,0:T(8,128)(2,1)}), bf16[8,64,2048]{2,1,0:T(8,128)(2,1)S(1)}, u32[]{:S(2)}, u32[]{:S(2)}) async-start(bf16[8,64,2048]{2,1,0:T(8,128)(2,1)} %bitcast.130), calls=%async_computation.6 | async-start | bytes 4194304 | tf_op jit(solution)/shard_map/all_to_all | solution.py:159
  245.7 46.2 %all-to-all-done.6 = bf16[8,64,2048]{2,1,0:T(8,128)(2,1)S(1)} async-done(((bf16[8,64,2048]{2,1,0:T(8,128)(2,1)}), bf16[8,64,2048]{2,1,0:T(8,128)(2,1)S(1)}, u32[]{:S(2)}, u32[]{:S(2)}) %all-to-all-start.6) | async-done | bytes 2097184 | tf_op jit(solution)/shard_map/all_to_all | solution.py:159
  291.9 1.4 gather_fusion
  293.3 1.3 reshape.290
  294.6 3.2 %multiply_reduce_fusion.2 = f32[128,2048]{1,0:T(8,128)S(1)} fusion(f32[128,2,2048]{2,1,0:T(2,128)S(1)} %reshape.290, f32[128,2]{1,0:T(8,128)S(1)} %copy.124), kind=kLoop, calls=%fused_computation.36 | loop fusion | flops 786432 | bytes 3146752 | tf_op jit(solution)/shard_map/reduce_sum | solution.py:165
  (86 shorter events, 23.9 us)
Async XLA Ops:
  9.4 9.1 %copy-start.3 = (bf16[1,128,16,128]{3,2,1,0:T(8,128)(2,1)S(1)}, bf16[1,128,16,128]{3,2,1,0:T(8,128)(2,1)}, u32[]{:S(2)}) copy-start(bf16[1,128,16,128]{3,2,1,0:T(8,128)(2,1)} %param.17) | copy-start | bytes 1572868
  9.4 9.5 %copy-start.8 = (f32[128]{0:T(128)S(1)}, f32[128]{0:T(128)}, u32[]{:S(2)}) copy-start(f32[128]{0:T(128)} %param.20) | copy-start | bytes 1540
  11.2 21.8 %all-to-all-start.1 = ((bf16[128,16,128]{2,0,1:T(8,128)(2,1)}), bf16[128,16,128]{2,0,1:T(8,128)(2,1)S(1)}, u32[]{:S(2)}, u32[]{:S(2)}) async-start(bf16[128,16,128]{2,0,1:T(8,128)(2,1)} %bitcast.12), calls=%async_computation.1 | async-start | bytes 1048576 | tf_op jit(solution)/shard_map/all_to_all | solution.py:112
  20.1 16.5 %copy-start.4 = (bf16[1,128,4,128]{3,2,1,0:T(4,128)(2,1)S(1)}, bf16[1,128,4,128]{3,2,1,0:T(4,128)(2,1)}, u32[]{:S(2)}) copy-start(bf16[1,128,4,128]{3,2,1,0:T(4,128)(2,1)} %param.19) | copy-start | bytes 393220
  33.0 18.3 %all-to-all-start = ((bf16[128,16,128]{2,0,1:T(8,128)(2,1)}), bf16[128,16,128]{2,0,1:T(8,128)(2,1)S(1)}, u32[]{:S(2)}, u32[]{:S(2)}) async-start(bf16[128,16,128]{2,0,1:T(8,128)(2,1)} %pad_maximum_fusion), calls=%async_computation | async-start | bytes 1048576 | tf_op jit(solution)/shard_map/all_to_all | solution.py:111
  52.2 18.3 %all-to-all-start.2 = ((bf16[128,16,128]{2,0,1:T(8,128)(2,1)}), bf16[128,16,128]{2,0,1:T(8,128)(2,1)S(1)}, u32[]{:S(2)}, u32[]{:S(2)}) async-start(bf16[128,16,128]{2,0,1:T(8,128)(2,1)} %bitcast.18), calls=%async_computation.2 | async-start | bytes 1048576 | tf_op jit(solution)/shard_map/all_to_all | solution.py:115
  55.8 57.9 %all-gather.5.cloned.1.call-start = ((), (), s32[]{:S(2)}) async-start(), calls=%async_computation.8 | async-start | bytes 2359296 | tf_op jit(solution)/shard_map/all_gather | solution.py:77
  56.6 80.3 %all-gather.3.cloned.1.call-start = ((), (), s32[]{:S(2)}) async-start(), calls=%async_computation.7 | async-start | bytes 2621440 | tf_op jit(solution)/shard_map/all_gather | solution.py:76
  106.2 1.4 copy-start.6
  141.1 12.3 %all-to-all-start.4 = ((bf16[4,128,512]{2,1,0:T(8,128)(2,1)}), bf16[4,128,512]{2,1,0:T(8,128)(2,1)S(1)}, u32[]{:S(2)}, u32[]{:S(2)}) async-start(bf16[4,128,512]{2,1,0:T(8,128)(2,1)} %fusion.29), calls=%async_computation.4 | async-start | bytes 1048576 | tf_op jit(solution)/shard_map/all_to_all | solution.py:81
  153.5 1.0 copy-start
  153.9 0.9 copy-start.5
  240.3 4.0 %copy-start.7 = (f32[1,128,2]{1,2,0:T(2,128)S(1)}, f32[1,128,2]{1,2,0:T(2,128)}, u32[]{:S(2)}) copy-start(f32[1,128,2]{1,2,0:T(2,128)} %param.29) | copy-start | bytes 3076
  240.3 51.6 %all-to-all-start.6 = ((bf16[8,64,2048]{2,1,0:T(8,128)(2,1)}), bf16[8,64,2048]{2,1,0:T(8,128)(2,1)S(1)}, u32[]{:S(2)}, u32[]{:S(2)}) async-start(bf16[8,64,2048]{2,1,0:T(8,128)(2,1)} %bitcast.130), calls=%async_computation.6 | async-start | bytes 4194304 | tf_op jit(solution)/shard_map/all_to_all | solution.py:159
  294.6 3.2 %copy-start.1 = (bf16[1,128,2048]{2,1,0:T(8,128)(2,1)S(1)}, bf16[1,128,2048]{2,1,0:T(8,128)(2,1)}, u32[]{:S(2)}) copy-start(bf16[1,128,2048]{2,1,0:T(8,128)(2,1)} %param.23) | copy-start | bytes 1572868
  294.6 3.2 %copy-start.2 = (f32[1,128,2048]{2,1,0:T(8,128)S(1)}, f32[1,128,2048]{2,1,0:T(8,128)}, u32[]{:S(2)}) copy-start(f32[1,128,2048]{2,1,0:T(8,128)} %copy.119) | copy-start | bytes 3145732
Sparse Core Ops, SparseCore 0:
  58.8 54.8 all-gather.4
  115.2 21.5 all-gather.2
where the time goes:
time: 306 us
  waiting for transfers between devices  123 us (40%)
  blocking collectives  81.4 us (27%)
  matrix products  35.4 us (12%)
  starting transfers between devices  22.2 us (7%)
  local copies, waits for them, and re-layouts  15.1 us (5%)
  other arithmetic  14.2 us (5%)
  between operations  13.8 us (5%)
    all_to_all x1, blocking collectives, on_device(): lax.all_to_all(buffer, 'sp', split_axis=0, concat_axis=0, tiled=True)  53.4 us
    all_to_all x1, waiting for transfers between devices, on_device(): lax.all_to_all(served, 'sp', split_axis=0, concat_axis=0, tiled=True)  46.2 us
    all_to_all x1, blocking collectives, on_device(): lax.all_to_all(by_heads, 'sp', split_axis=0, concat_axis=1, tiled=True)  28 us
    all_gather x1, waiting for transfers between devices, project_tokens(): all_rows = lax.all_gather(attended[None], 'dp', axis=0, tiled=True)  23.2 us
    dot_general x1, matrix products, on_device(): jnp.dot(hidden, expert_down[0], preferred_element_type=jnp.float32)  17 us
    all_to_all x1, waiting for transfers between devices, on_device(): lax.all_to_all(rot_query, 'sp', split_axis=1, concat_axis=0, tiled=True)  14.6 us
    all_to_all x1, waiting for transfers between devices, on_device(): lax.all_to_all(jnp.repeat(value_rows, group_size, axis=1), 'sp', split_ax...  13.7 us
    all_to_all x1, waiting for transfers between devices, on_device(): lax.all_to_all(jnp.repeat(rot_key, group_size, axis=1), 'sp', split_axis=...  11.4 us
  transfers between devices with their start and end apart: 7, of which 7 were waited for; matrix products, arithmetic and copies ran while one was open for 5% of the time, Pallas kernels for 0%

commit v1 on v0

--- a/solution.py
+++ b/solution.py
@@ -6,6 +6,32 @@
 GRID_W = 64
 EPS = 1e-06
 THETA = 10000.0
+
+
+def ring_apply(value, axis, dim, work, out_dim):
+    size, mine, width = (lax.axis_size(axis), lax.axis_index(axis), value.shape[dim])
+    forward = [(i, (i + 1) % size) for i in range(size)]
+    behind = [(b, a) for a, b in forward]
+    lower, upper = (lax.ppermute(value, axis, forward), lax.ppermute(value, axis, behind))
+    made = work(value, mine * width)
+    length = made.shape[out_dim]
+    filled = jnp.zeros(
+        (*made.shape[:out_dim], size * length, *made.shape[out_dim + 1 :]), made.dtype
+    )
+
+    def put(filled, made, owner):
+        return lax.dynamic_update_slice_in_dim(filled, made, owner * length, axis=out_dim)
+
+    filled = put(filled, made, mine)
+    for step in range(1, size // 2 + 1):
+        below, above = ((mine - step) % size, (mine + step) % size)
+        held = (lower, upper)
+        if step < size // 2:
+            lower, upper = (lax.ppermute(lower, axis, forward), lax.ppermute(upper, axis, behind))
+        filled = put(filled, work(held[0], below * width), below)
+        if 2 * step < size:
+            filled = put(filled, work(held[1], above * width), above)
+    return filled
 
 
 def rotate_half(vector, position):
@@ -73,10 +99,15 @@
 
 
 def project_tokens(attended, out_weight):
-    all_rows = lax.all_gather(attended[None], "dp", axis=0, tiled=True)
     local_cols = lax.all_gather(out_weight, "sp", axis=0, tiled=True)
-    partial_cols = jnp.einsum(
-        "std,dc->stc", all_rows, local_cols, preferred_element_type=jnp.float32
+    partial_cols = ring_apply(
+        attended[None],
+        "dp",
+        0,
+        lambda shard, start: jnp.einsum(
+            "std,dc->stc", shard, local_cols, preferred_element_type=jnp.float32
+        ),
+        0,
     )
     back_cols = lax.all_to_all(
         partial_cols.astype(jnp.bfloat16), "dp", split_axis=0, concat_axis=2, tiled=True

time: 306 us -> 293 us (0.958)
  blocking collectives: 81.4 us -> 52.9 us
  waiting for transfers between devices: 123 us -> 131 us
  starting transfers between devices: 22.2 us -> 28.2 us
    all_to_all x1 -> x0, blocking collectives: 28 us -> none  [on_device(): lax.all_to_all(by_heads, 'sp', split_axis=0, concat_axis=1, tiled=True)]
    all_to_all x0 -> x1, waiting for transfers between devices: none -> 24 us  [on_device(): lax.all_to_all(by_heads, 'sp', split_axis=0, concat_axis=1, tiled=True)]
    all_gather x1 -> x0, waiting for transfers between devices: 23.2 us -> none  [project_tokens(): all_rows = lax.all_gather(attended[None], 'dp', axis=0, tiled=True)]
    ppermute x0 -> x3, waiting for transfers between devices: none -> 11.4 us  [the longest x1 8.89 us: ring_apply(): lax.ppermute(value, axis, forward)]
    all_gather x1, waiting for transfers between devices: 5.06 us -> 0.01 us  [project_tokens(): local_cols = lax.all_gather(out_weight, 'sp', axis=0, tiled=True)]
    all_to_all x0 -> x1, starting transfers between devices: none -> 3.63 us  [on_device(): lax.all_to_all(by_heads, 'sp', split_axis=0, concat_axis=1, tiled=True)]
  transfers between devices with their start and end apart: 7 -> 10, of which waited for: 7 -> 8; matrix products, arithmetic and copies ran while one was open for 5% -> 7% of each run, Pallas kernels for 0% -> 0%
where the time goes in v1:
time: 293 us
  waiting for transfers between devices  131 us (45%)
  blocking collectives  52.9 us (18%)
  matrix products  37.2 us (13%)
  starting transfers between devices  28.2 us (10%)
  local copies, waits for them, and re-layouts  15.7 us (5%)
  other arithmetic  14.2 us (5%)
  between operations  13.9 us (5%)
    all_to_all x1, blocking collectives, on_device(): lax.all_to_all(buffer, 'sp', split_axis=0, concat_axis=0, tiled=True)  52.9 us
    all_to_all x1, waiting for transfers between devices, on_device(): lax.all_to_all(served, 'sp', split_axis=0, concat_axis=0, tiled=True)  46 us
    all_to_all x1, waiting for transfers between devices, on_device(): lax.all_to_all(by_heads, 'sp', split_axis=0, concat_axis=1, tiled=True)  24 us
    dot_general x1, matrix products, on_device(): jnp.dot(hidden, expert_down[0], preferred_element_type=jnp.float32)  17 us
    all_to_all x1, waiting for transfers between devices, on_device(): lax.all_to_all(rot_query, 'sp', split_axis=1, concat_axis=0, tiled=True)  14.6 us
    all_to_all x1, waiting for transfers between devices, on_device(): lax.all_to_all(jnp.repeat(value_rows, group_size, axis=1), 'sp', split_ax...  13.7 us
    all_to_all x1, waiting for transfers between devices, on_device(): lax.all_to_all(jnp.repeat(rot_key, group_size, axis=1), 'sp', split_axis=...  11.4 us
    dot_general x1, matrix products, on_device(): jnp.dot(flat_rows, expert_gate[0], preferred_element_type=jnp.float32)  9.45 us
  transfers between devices with their start and end apart: 10, of which 8 were waited for; matrix products, arithmetic and copies ran while one was open for 7% of the time, Pallas kernels for 0%

profile of v1, /device:TPU:0, one launch (start us, length us, event | category | flops | bytes accessed | tf_op | source)
XLA Modules:
  0.0 292.7 jit_solution(8233414892247400450)
XLA Ops:
  11.2 7.3 %all-to-all-start.1 = ((bf16[128,16,128]{2,0,1:T(8,128)(2,1)}), bf16[128,16,128]{2,0,1:T(8,128)(2,1)S(1)}, u32[]{:S(2)}, u32[]{:S(2)}) async-start(bf16[128,16,128]{2,0,1:T(8,128)(2,1)} %bitcast.12), calls=%async_computation.1 | async-start | bytes 1048576 | tf_op jit(solution)/shard_map/all_to_all | solution.py:143
  20.1 1.5 pad_maximum_fusion
  21.6 11.4 %all-to-all-done.1 = bf16[128,16,128]{2,0,1:T(8,128)(2,1)S(1)} async-done(((bf16[128,16,128]{2,0,1:T(8,128)(2,1)}), bf16[128,16,128]{2,0,1:T(8,128)(2,1)S(1)}, u32[]{:S(2)}, u32[]{:S(2)}) %all-to-all-start.1) | async-done | bytes 524320 | tf_op jit(solution)/shard_map/all_to_all | solution.py:143
  33.0 3.6 %all-to-all-start = ((bf16[128,16,128]{2,0,1:T(8,128)(2,1)}), bf16[128,16,128]{2,0,1:T(8,128)(2,1)S(1)}, u32[]{:S(2)}, u32[]{:S(2)}) async-start(bf16[128,16,128]{2,0,1:T(8,128)(2,1)} %pad_maximum_fusion), calls=%async_computation | async-start | bytes 1048576 | tf_op jit(solution)/shard_map/all_to_all | solution.py:142
  36.7 14.6 %all-to-all-done = bf16[128,16,128]{2,0,1:T(8,128)(2,1)S(1)} async-done(((bf16[128,16,128]{2,0,1:T(8,128)(2,1)}), bf16[128,16,128]{2,0,1:T(8,128)(2,1)S(1)}, u32[]{:S(2)}, u32[]{:S(2)}) %all-to-all-start) | async-done | bytes 524320 | tf_op jit(solution)/shard_map/all_to_all | solution.py:142
  52.2 3.6 %all-to-all-start.2 = ((bf16[128,16,128]{2,0,1:T(8,128)(2,1)}), bf16[128,16,128]{2,0,1:T(8,128)(2,1)S(1)}, u32[]{:S(2)}, u32[]{:S(2)}) async-start(bf16[128,16,128]{2,0,1:T(8,128)(2,1)} %bitcast.18), calls=%async_computation.2 | async-start | bytes 1048576 | tf_op jit(solution)/shard_map/all_to_all | solution.py:146
  56.7 13.7 %all-to-all-done.2 = bf16[128,16,128]{2,0,1:T(8,128)(2,1)S(1)} async-done(((bf16[128,16,128]{2,0,1:T(8,128)(2,1)}), bf16[128,16,128]{2,0,1:T(8,128)(2,1)S(1)}, u32[]{:S(2)}, u32[]{:S(2)}) %all-to-all-start.2) | async-done | bytes 524320 | tf_op jit(solution)/shard_map/all_to_all | solution.py:146
  70.6 3.4 %while.20 = (s32[]{:T(128)}, bf16[2,512,128]{2,1,0:T(8,128)(2,1)S(1)}, bf16[2,512,128]{2,1,0:T(8,128)(2,1)S(1)}, bf16[1024,128]{1,0:T(8,128)(2,1)S(1)}, bf16[1024,128]{1,0:T(8,128)(2,1)S(1)}, /*index=5*/s32[]{:T(128)}) while((s32[]{:T(128)}, bf16[2,512,128]{2,1,0:T(8,128)(2,1)S(1)}, bf16[2,512,128]{2,1,0:T(8,128)(2,1)S(1)}, ...), condition=%wide.region_5.6_spmd, body=%wide.region_2.5_spmd.sunk | while | flops 273218560 | bytes 7088205 | solution.py:97
  74.1 3.5 %while.21 = (s32[]{:T(128)}, bf16[2,512,128]{2,1,0:T(8,128)(2,1)S(1)}, bf16[2,512,128]{2,1,0:T(8,128)(2,1)S(1)}, bf16[1024,128]{1,0:T(8,128)(2,1)S(1)}, bf16[1024,128]{1,0:T(8,128)(2,1)S(1)}, /*index=5*/s32[]{:T(128)}) while((s32[]{:T(128)}, bf16[2,512,128]{2,1,0:T(8,128)(2,1)S(1)}, bf16[2,512,128]{2,1,0:T(8,128)(2,1)S(1)}, ...), condition=%wide.region_9.10_spmd, body=%wide.region_6.9_spmd.sunk | while | flops 273218560 | bytes 7088205 | solution.py:97
  79.0 3.6 %all-to-all-start.3 = ((bf16[1024,2,128]{2,1,0:T(2,128)(2,1)}), bf16[1024,2,128]{2,1,0:T(2,128)(2,1)S(1)}, u32[]{:S(2)}, u32[]{:S(2)}) async-start(bf16[1024,2,128]{2,1,0:T(2,128)(2,1)} %copy.111), calls=%async_computation.3 | async-start | bytes 1048576 | tf_op jit(solution)/shard_map/all_to_all | solution.py:155
  82.9 24.0 %all-to-all-done.3 = bf16[1024,2,128]{2,1,0:T(2,128)(2,1)S(1)} async-done(((bf16[1024,2,128]{2,1,0:T(2,128)(2,1)}), bf16[1024,2,128]{2,1,0:T(2,128)(2,1)S(1)}, u32[]{:S(2)}, u32[]{:S(2)}) %all-to-all-start.3) | async-done | bytes 524320 | tf_op jit(solution)/shard_map/all_to_all | solution.py:155
  108.1 1.8 collective-permute-start.1
  109.9 8.9 %collective-permute-done = bf16[1,128,2048]{1,2,0:T(8,128)(2,1)S(1)} collective-permute-done((bf16[1,128,2048]{1,2,0:T(8,128)(2,1)S(1)}, bf16[1,128,2048]{1,2,0:T(8,128)(2,1)S(1)}, u32[]{:S(2)}, u32[]{:S(2)}) %collective-permute-start) | collective-permute-done | bytes 524320 | tf_op jit(solution)/shard_map/ppermute | solution.py:15
  119.9 2.7 fusion.30
  124.9 2.5 collective-permute-done.2
  128.5 3.9 %all-to-all-start.4 = ((bf16[4,128,512]{2,1,0:T(8,128)(2,1)}), bf16[4,128,512]{2,1,0:T(8,128)(2,1)S(1)}, u32[]{:S(2)}, u32[]{:S(2)}) async-start(bf16[4,128,512]{2,1,0:T(8,128)(2,1)} %fusion.27), calls=%async_computation.4 | async-start | bytes 1048576 | tf_op jit(solution)/shard_map/all_to_all | solution.py:112
  132.5 8.7 %all-to-all-done.4 = bf16[4,128,512]{2,1,0:T(8,128)(2,1)S(1)} async-done(((bf16[4,128,512]{2,1,0:T(8,128)(2,1)}), bf16[4,128,512]{2,1,0:T(8,128)(2,1)S(1)}, u32[]{:S(2)}, u32[]{:S(2)}) %all-to-all-start.4) | async-done | bytes 524320 | tf_op jit(solution)/shard_map/all_to_all | solution.py:112
  144.7 3.5 %scatter_custom_fusion = bf16[512,2048]{1,0:T(8,128)(2,1)S(1)} fusion(s32[256]{0:T(256)S(1)} %bitcast.169, bf16[256,2048]{1,0:T(8,128)(2,1)} %reshape.326, bf16[]{:T(256)} %constant.115.clone.1), kind=kCustom, calls=%fused_computation.55 | custom fusion | bytes 2097664 | tf_op jit(solution)/shard_map/scatter | solution.py:177
  148.2 52.9 %all_to_all.88 = bf16[8,64,2048]{2,1,0:T(8,128)(2,1)} all-to-all(bf16[8,64,2048]{2,1,0:T(8,128)(2,1)S(1)} %bitcast.152), channel_id=1, replica_groups=mesh['sp'=8,'dp'=4] {'sp'}, dimensions={0} | all-to-all | bytes 4194304 | tf_op jit(solution)/shard_map/all_to_all | solution.py:180
  201.1 9.5 %fusion.20 = f32[512,1792]{1,0:T(8,128)} fusion(bf16[512,2048]{1,0:T(8,128)(2,1)} %bitcast.49, bf16[1,2048,1792]{2,1,0:T(8,128)(2,1)} %param.25), kind=kOutput, calls=%fused_computation.30 | convolution fusion | flops 3758096384 | bytes 13107200 | tf_op jit(solution)/shard_map/dot_general | solution.py:183
  210.6 17.0 %fusion.24 = bf16[512,2048]{1,0:T(8,128)(2,1)} fusion(bf16[1,1792,2048]{2,1,0:T(8,128)(2,1)} %param.27, f32[512,1792]{1,0:T(8,128)} %fusion.20, bf16[512,2048]{1,0:T(8,128)(2,1)} %bitcast.49, bf16[1,2048,1792]{2,1,0:T(8,128)(2,1)} %param.26), kind=kOutput, calls=%fused_computation.33 | convolution fusion | flops 7522746368 | bytes 22544384 | tf_op jit(solution)/shard_map/dot_general | solution.py:186
  227.5 4.0 %all-to-all-start.6 = ((bf16[8,64,2048]{2,1,0:T(8,128)(2,1)}), bf16[8,64,2048]{2,1,0:T(8,128)(2,1)S(1)}, u32[]{:S(2)}, u32[]{:S(2)}) async-start(bf16[8,64,2048]{2,1,0:T(8,128)(2,1)} %bitcast.155), calls=%async_computation.6 | async-start | bytes 4194304 | tf_op jit(solution)/shard_map/all_to_all | solution.py:190
  232.9 46.0 %all-to-all-done.6 = bf16[8,64,2048]{2,1,0:T(8,128)(2,1)S(1)} async-done(((bf16[8,64,2048]{2,1,0:T(8,128)(2,1)}), bf16[8,64,2048]{2,1,0:T(8,128)(2,1)S(1)}, u32[]{:S(2)}, u32[]{:S(2)}) %all-to-all-start.6) | async-done | bytes 2097184 | tf_op jit(solution)/shard_map/all_to_all | solution.py:190
  281.7 3.2 %multiply_reduce_fusion.2 = f32[128,2048]{1,0:T(8,128)S(1)} fusion(f32[128,2,2048]{2,1,0:T(2,128)S(1)} %reshape.311, f32[128,2]{1,0:T(8,128)S(1)} %copy.121), kind=kLoop, calls=%fused_computation.34 | loop fusion | flops 786432 | bytes 3146752 | tf_op jit(solution)/shard_map/reduce_sum | solution.py:196
  (95 shorter events, 30.8 us)
Async XLA Ops:
  9.4 9.1 %copy-start.4 = (bf16[1,128,16,128]{3,2,1,0:T(8,128)(2,1)S(1)}, bf16[1,128,16,128]{3,2,1,0:T(8,128)(2,1)}, u32[]{:S(2)}) copy-start(bf16[1,128,16,128]{3,2,1,0:T(8,128)(2,1)} %param.17) | copy-start | bytes 1572868
  9.4 9.5 %copy-start.9 = (f32[128]{0:T(128)S(1)}, f32[128]{0:T(128)}, u32[]{:S(2)}) copy-start(f32[128]{0:T(128)} %param.20) | copy-start | bytes 1540
  11.2 21.8 %all-to-all-start.1 = ((bf16[128,16,128]{2,0,1:T(8,128)(2,1)}), bf16[128,16,128]{2,0,1:T(8,128)(2,1)S(1)}, u32[]{:S(2)}, u32[]{:S(2)}) async-start(bf16[128,16,128]{2,0,1:T(8,128)(2,1)} %bitcast.12), calls=%async_computation.1 | async-start | bytes 1048576 | tf_op jit(solution)/shard_map/all_to_all | solution.py:143
  20.1 16.5 %copy-start.5 = (bf16[1,128,4,128]{3,2,1,0:T(4,128)(2,1)S(1)}, bf16[1,128,4,128]{3,2,1,0:T(4,128)(2,1)}, u32[]{:S(2)}) copy-start(bf16[1,128,4,128]{3,2,1,0:T(4,128)(2,1)} %param.19) | copy-start | bytes 393220
  33.0 18.3 %all-to-all-start = ((bf16[128,16,128]{2,0,1:T(8,128)(2,1)}), bf16[128,16,128]{2,0,1:T(8,128)(2,1)S(1)}, u32[]{:S(2)}, u32[]{:S(2)}) async-start(bf16[128,16,128]{2,0,1:T(8,128)(2,1)} %pad_maximum_fusion), calls=%async_computation | async-start | bytes 1048576 | tf_op jit(solution)/shard_map/all_to_all | solution.py:142
  52.2 18.3 %all-to-all-start.2 = ((bf16[128,16,128]{2,0,1:T(8,128)(2,1)}), bf16[128,16,128]{2,0,1:T(8,128)(2,1)S(1)}, u32[]{:S(2)}, u32[]{:S(2)}) async-start(bf16[128,16,128]{2,0,1:T(8,128)(2,1)} %bitcast.18), calls=%async_computation.2 | async-start | bytes 1048576 | tf_op jit(solution)/shard_map/all_to_all | solution.py:146
  55.8 63.2 %all-gather.2.cloned.1.call-start = ((), (), s32[]{:S(2)}) async-start(), calls=%async_computation.7 | async-start | bytes 2359296 | tf_op jit(solution)/shard_map/all_gather | solution.py:102
  77.6 5.0 %copy-start.7 = (s32[1,128,2]{1,2,0:T(2,128)S(1)}, s32[1,128,2]{1,2,0:T(2,128)}, u32[]{:S(2)}) copy-start(s32[1,128,2]{1,2,0:T(2,128)} %param.28) | copy-start | bytes 3076
  79.0 27.9 %all-to-all-start.3 = ((bf16[1024,2,128]{2,1,0:T(2,128)(2,1)}), bf16[1024,2,128]{2,1,0:T(2,128)(2,1)S(1)}, u32[]{:S(2)}, u32[]{:S(2)}) async-start(bf16[1024,2,128]{2,1,0:T(2,128)(2,1)} %copy.111), calls=%async_computation.3 | async-start | bytes 1048576 | tf_op jit(solution)/shard_map/all_to_all | solution.py:155
  107.2 11.6 %collective-permute-start = (bf16[1,128,2048]{1,2,0:T(8,128)(2,1)S(1)}, bf16[1,128,2048]{1,2,0:T(8,128)(2,1)S(1)}, u32[]{:S(2)}, u32[]{:S(2)}) collective-permute-start(bf16[1,128,2048]{1,2,0:T(8,128)(2,1)S(1)} %bitcast.163), channel_id=1, source_target_pairs={{0,1},{1,2},{2,3},{3,0},{4,5},{5,6},{6,7},{7,4},{8,9},{9,10},{10,1... | collective-permute-start | bytes 1572872 | tf_op jit(solution)/shard_map/ppermute | solution.py:15
  108.1 15.6 %collective-permute-start.1 = (bf16[1,128,2048]{1,2,0:T(8,128)(2,1)S(1)}, bf16[1,128,2048]{1,2,0:T(8,128)(2,1)S(1)}, u32[]{:S(2)}, u32[]{:S(2)}) collective-permute-start(bf16[1,128,2048]{1,2,0:T(8,128)(2,1)S(1)} %bitcast.164), channel_id=1, source_target_pairs={{1,0},{2,1},{3,2},{0,3},{5,4},{6,5},{7,6},{4,7},{9,8},{10,9},{11,1... | collective-permute-start | bytes 1572872 | tf_op jit(solution)/shard_map/ppermute | solution.py:15
  118.8 8.6 %collective-permute-start.2 = (bf16[1,128,2048]{1,2,0:T(8,128)(2,1)S(1)}, bf16[1,128,2048]{1,2,0:T(8,128)(2,1)S(1)}, u32[]{:S(2)}, u32[]{:S(2)}) collective-permute-start(bf16[1,128,2048]{1,2,0:T(8,128)(2,1)S(1)} %collective-permute-done), channel_id=1, source_target_pairs={{0,1},{1,2},{2,3},{3,0},{4,5},{5,6},{6,7},{7,4},{8,9},{9,10},{10,1... | collective-permute-start | bytes 1572872 | tf_op jit(solution)/shard_map/ppermute | solution.py:30
  119.0 3.6 %copy-start = (bf16[2048,512]{1,0:T(8,128)(2,1)S(1)}, bf16[2048,512]{1,0:T(8,128)(2,1)}, u32[]{:S(2)}) copy-start(bf16[2048,512]{1,0:T(8,128)(2,1)} %all-gather.2.cloned.1.call-done) | copy-start | bytes 6291460
  128.5 12.7 %all-to-all-start.4 = ((bf16[4,128,512]{2,1,0:T(8,128)(2,1)}), bf16[4,128,512]{2,1,0:T(8,128)(2,1)S(1)}, u32[]{:S(2)}, u32[]{:S(2)}) async-start(bf16[4,128,512]{2,1,0:T(8,128)(2,1)} %fusion.27), calls=%async_computation.4 | async-start | bytes 1048576 | tf_op jit(solution)/shard_map/all_to_all | solution.py:112
  141.3 1.0 copy-start.1
  141.7 0.9 copy-start.6
  227.5 4.0 %copy-start.8 = (f32[1,128,2]{1,2,0:T(2,128)S(1)}, f32[1,128,2]{1,2,0:T(2,128)}, u32[]{:S(2)}) copy-start(f32[1,128,2]{1,2,0:T(2,128)} %param.29) | copy-start | bytes 3076
  227.5 51.4 %all-to-all-start.6 = ((bf16[8,64,2048]{2,1,0:T(8,128)(2,1)}), bf16[8,64,2048]{2,1,0:T(8,128)(2,1)S(1)}, u32[]{:S(2)}, u32[]{:S(2)}) async-start(bf16[8,64,2048]{2,1,0:T(8,128)(2,1)} %bitcast.155), calls=%async_computation.6 | async-start | bytes 4194304 | tf_op jit(solution)/shard_map/all_to_all | solution.py:190
  281.6 3.2 %copy-start.2 = (bf16[1,128,2048]{2,1,0:T(8,128)(2,1)S(1)}, bf16[1,128,2048]{2,1,0:T(8,128)(2,1)}, u32[]{:S(2)}) copy-start(bf16[1,128,2048]{2,1,0:T(8,128)(2,1)} %param.23) | copy-start | bytes 1572868
  281.7 3.2 %copy-start.3 = (f32[1,128,2048]{2,1,0:T(8,128)S(1)}, f32[1,128,2048]{2,1,0:T(8,128)}, u32[]{:S(2)}) copy-start(f32[1,128,2048]{2,1,0:T(8,128)} %copy.116) | copy-start | bytes 3145732
Sparse Core Ops, SparseCore 0:
  58.8 55.8 all-gather.1
